TPU v7x, 32 devices: a whole 2x2x4 slice. The times are simulated.
32 devices in a mesh: grp: 2 (over y), sp: 4 (over z), tp: 4 (over x, core).
Axes of the slice: x: 2, y: 2, z: 4, core: 2. Of those that a mesh axis runs over, the one named last changes fastest.
Arguments:
- target: bfloat16 [1024, 2048], P(('grp', 'sp', 'tp')), parts along dimension 0, may hold values from -60 to 60
- source: bfloat16 [8192, 2048], P(('grp', 'sp', 'tp')), parts along dimension 0, may hold values from -120 to 120
- w_query: bfloat16 [2, 2048, 2048], P(None, None, 'tp'), may hold values from -0.176776695 to 0.176776695
- w_key: bfloat16 [2, 2048, 2048], P(None, None, 'tp'), may hold values from -0.176776695 to 0.176776695
- w_value: bfloat16 [2, 2048, 2048], P(None, None, 'tp'), may hold values from -0.125 to 0.125
- w_out: bfloat16 [2, 2048, 2048], P(None, 'tp'), may hold values from -0.125 to 0.125
- gains: float32 [2, 2, 2048], replicated, may hold values from 0.1 to 1.9
Outputs:
- mixed: bfloat16 [1024, 2048], P(('grp', 'sp', 'tp')), parts along dimension 0
There are 2 independent parts, one for each index of `grp`. A program takes and returns all parts, laid end to end along the dimension named above; an argument that names none is the same for every part. Nothing has to cross between parts.
All inputs are finite; a program needn't handle non-finite values.
Results may differ from a plain program's by a relative error of at most 0.025.
Values may be sent and summed in bfloat16 or wider, within the bound.
A program may use at most 128 MiB of HBM per device.

v0:
```python
import jax
import jax.numpy as jnp
from jax import lax
from jax.sharding import PartitionSpec as P

HEAD = 128


EPS = 1e-06


def normalize(row_block, gain_row):
    return (
        row_block
        * lax.rsqrt(jnp.mean(row_block * row_block, axis=-1, keepdims=True) + EPS)
        * gain_row
    )


def split_heads(row_block):
    return row_block.reshape(row_block.shape[0], row_block.shape[1] // HEAD, HEAD)


def body(target, source, w_query, w_key, w_value, w_out, gains):
    local_width = w_query.shape[2]
    score_scale = HEAD ** (-0.5)
    depth = w_query.shape[0]
    project_shard_part = lax.all_gather(source, "tp", axis=0, tiled=True)
    layer_parts = [
        jnp.stack(
            [
                jnp.dot(project_shard_part, w_key[level], preferred_element_type=jnp.float32),
                jnp.dot(project_shard_part, w_value[level], preferred_element_type=jnp.float32),
            ]
        )
        for level in range(depth)
    ]
    projected_source = jnp.stack(layer_parts).astype(jnp.bfloat16)
    stream = target.astype(jnp.float32)
    for layer_index in range(depth):
        normed = normalize(stream, gains[layer_index, 0]).astype(jnp.bfloat16)
        query_weight = w_query[layer_index]
        queries = jnp.dot(
            lax.all_gather(normed, "tp", axis=0, tiled=True),
            query_weight,
            preferred_element_type=jnp.float32,
        ).astype(jnp.bfloat16)
        row_count = queries.shape[0]
        keys_here = projected_source[layer_index, 0]
        values_here = projected_source[layer_index, 1]
        every_query = lax.all_gather(queries, "sp", axis=0, tiled=True)
        scores = (
            jnp.einsum(
                "qhd,khd->hqk",
                split_heads(every_query),
                split_heads(keys_here),
                preferred_element_type=jnp.float32,
            )
            * score_scale
        )
        row_peak = lax.pmax(jnp.max(scores, axis=2), "sp")
        weights = jnp.exp(scores - row_peak[:, :, None])
        local_summed = jnp.einsum(
            "hqk,khd->hqd",
            weights.astype(jnp.bfloat16),
            split_heads(values_here),
            preferred_element_type=jnp.float32,
        )
        summed, row_total = (
            lax.psum_scatter(
                local_summed.astype(jnp.bfloat16), "sp", scatter_dimension=1, tiled=True
            ).astype(jnp.float32),
            lax.psum_scatter(
                jnp.sum(weights, axis=2).astype(jnp.bfloat16), "sp", scatter_dimension=1, tiled=True
            ).astype(jnp.float32),
        )
        heads_out = summed / row_total[:, :, None]
        attended = (
            jnp.transpose(heads_out, (1, 0, 2)).reshape(row_count, local_width).astype(jnp.bfloat16)
        )
        out_weight = w_out[layer_index]
        projected = lax.psum_scatter(
            jnp.dot(attended, out_weight, preferred_element_type=jnp.float32).astype(jnp.bfloat16),
            "tp",
            scatter_dimension=0,
            tiled=True,
        ).astype(jnp.float32)
        stream = stream + normalize(projected, gains[layer_index, 1])
    return stream.astype(jnp.bfloat16)


def solution(mesh):
    in_specs = (
        P(("grp", "sp", "tp"), None),
        P(("grp", "sp", "tp"), None),
        P(None, None, "tp"),
        P(None, None, "tp"),
        P(None, None, "tp"),
        P(None, "tp", None),
        P(),
    )
    out_specs = P(("grp", "sp", "tp"), None)
    return jax.shard_map(body, mesh=mesh, in_specs=in_specs, out_specs=out_specs, check_vma=False)
```

profile of v0, /device:TPU:0, one launch (start us, length us, event | category | flops | bytes accessed | tf_op | source)
XLA Modules:
  0.0 262.3 jit_solution(11381549648097681641)
XLA Ops:
  10.2 8.6 %all_gather.15 = bf16[128,2048]{1,0:T(8,128)(2,1)S(1)} all-gather(bf16[32,2048]{1,0:T(8,128)(2,1)S(1)} %fusion.84), channel_id=1, replica_groups=mesh['grp'=2,'sp'=4,'tp'=4] {'tp'}, dimensions={0}, use_global_device_ids=true | all-gather | bytes 655360 | tf_op jit(solution)/shard_map/all_gather | solution.py:44
  21.1 16.3 %all_gather.16 = bf16[512,512]{1,0:T(8,128)(2,1)S(1)} all-gather(bf16[128,512]{1,0:T(8,128)(2,1)S(1)} %fusion.64), channel_id=1, replica_groups=mesh['grp'=2,'sp'=4,'tp'=4] {'sp'}, dimensions={0}, use_global_device_ids=true | all-gather | bytes 655360 | tf_op jit(solution)/shard_map/all_gather | solution.py:51
  37.4 8.7 %all-gather.2.cloned.1.call-done = bf16[1024,2048]{1,0:T(8,128)(2,1)} async-done(((bf16[256,2048]{1,0:T(8,128)(2,1)}), bf16[1024,2048]{1,0:T(8,128)(2,1)}) %all-gather.2.cloned.1.call-update) | async-done | bytes 4194320 | tf_op jit(solution)/shard_map/all_gather | solution.py:28
  46.1 5.4 %fusion.52 = bf16[1,1024,512]{1,2,0:T(8,128)(2,1)S(1)} fusion(bf16[1024,2048]{1,0:T(8,128)(2,1)} %all-gather.2.cloned.1.call-done, bf16[2,2048,512]{2,1,0:T(8,128)(2,1)} %param.11), kind=kOutput, calls=%fused_computation.46 | convolution fusion | flops 2148007936 | bytes 7340032 | tf_op jit(solution)/shard_map/dot_general | solution.py:33
  54.3 4.5 %multiply_reduce_fusion.1 = (f32[4,512]{1,0:T(4,128)S(1)}, f32[4,512,1024]{2,1,0:T(8,128)}) fusion(bf16[1024,4,128]{0,2,1:T(8,128)(2,1)S(1)} %bitcast.105, bf16[512,512]{1,0:T(8,128)(2,1)S(1)} %all_gather.16), kind=kOutput, calls=%fused_computation.3 | convolution fusion | flops 541063168 | bytes 9969664 | tf_op jit(solution)/shard_map/qhd,khd->hqk/dot_general | solution.py:53
  58.8 11.8 %pmax.14 = f32[4,512]{1,0:T(4,128)S(1)} all-reduce(f32[4,512]{1,0:T(4,128)S(1)} %get-tuple-element.13), channel_id=1, replica_groups=mesh['grp'=2,'sp'=4,'tp'=4] {'sp'}, use_global_device_ids=true, to_apply=%region_2.0 | all-reduce | flops 2048 | bytes 16384 | tf_op jit(solution)/shard_map/pmax | solution.py:61
  70.6 4.4 %fusion = bf16[4,512]{1,0:T(4,128)(2,1)S(1)} fusion(f32[4,512,1024]{2,1,0:T(8,128)} %get-tuple-element.14, f32[4,512]{1,0:T(4,128)S(1)} %pmax.14), kind=kLoop, calls=%fused_computation.4 | loop fusion | flops 6289408 | bytes 8400896 | tf_op jit(solution)/shard_map/reduce_sum | solution.py:74
  75.9 5.7 %fusion.58 = bf16[4,512,128]{2,1,0:T(8,128)(2,1)} fusion(bf16[1024,4,128]{0,2,1:T(8,128)(2,1)S(1)} %bitcast.107, f32[4,512,1024]{2,1,0:T(8,128)} %get-tuple-element.14, f32[4,512]{1,0:T(4,128)S(1)} %pmax.14), kind=kOutput, calls=%fused_computation.48 | convolution fusion | flops 543424512 | bytes 9969664 | tf_op jit(solution)/shard_map/hqk,khd->hqd/dot_general | solution.py:63
  81.9 5.2 %fusion.46 = bf16[1,1024,512]{1,2,0:T(8,128)(2,1)S(1)} fusion(bf16[1024,2048]{1,0:T(8,128)(2,1)} %all-gather.2.cloned.1.call-done, bf16[2,2048,512]{2,1,0:T(8,128)(2,1)} %param.11), kind=kOutput, calls=%fused_computation.44 | convolution fusion | flops 2148007936 | bytes 7340032 | tf_op jit(solution)/shard_map/dot_general | solution.py:33
  87.1 5.5 %reduce-scatter.19.cloned.1.call-done = bf16[128,4]{1,0:T(8,128)(2,1)} async-done(((bf16[512,4]{1,0:T(8,128)(2,1)}), bf16[128,4]{1,0:T(8,128)(2,1)}) %reduce-scatter.19.cloned.1.call-update) | async-done | bytes 1040
  93.5 21.5 %reduce-scatter.11.cloned.1.call-done = bf16[4,128,128]{2,1,0:T(8,128)(2,1)} async-done(((bf16[4,512,128]{2,1,0:T(8,128)(2,1)}), bf16[4,128,128]{2,1,0:T(8,128)(2,1)}) %reduce-scatter.11.cloned.1.call-update) | async-done | bytes 131088 | tf_op jit(solution)/shard_map/reduce_scatter | solution.py:70
  116.2 2.9 %convolution_convert_fusion.1 = bf16[128,2048]{1,0:T(8,128)(2,1)} fusion(bf16[128,512]{0,1:T(8,128)(2,1)S(1)} %bitcast.110, bf16[2,512,2048]{2,1,0:T(8,128)(2,1)} %param.12), kind=kOutput, calls=%fused_computation.15 | convolution fusion | flops 268697600 | bytes 2752512 | tf_op jit(solution)/shard_map/dot_general | solution.py:83
  119.1 5.2 %fusion.49 = bf16[1,1024,512]{1,2,0:T(8,128)(2,1)S(1)} fusion(bf16[1024,2048]{1,0:T(8,128)(2,1)} %all-gather.2.cloned.1.call-done, bf16[2,2048,512]{2,1,0:T(8,128)(2,1)} %param.10), kind=kOutput, calls=%fused_computation.45 | convolution fusion | flops 2148007936 | bytes 7340032 | tf_op jit(solution)/shard_map/dot_general | solution.py:32
  124.8 14.4 %reduce-scatter.13.cloned.1.call-done = bf16[32,2048]{1,0:T(8,128)(2,1)} async-done(((bf16[128,2048]{1,0:T(8,128)(2,1)}), bf16[32,2048]{1,0:T(8,128)(2,1)}) %reduce-scatter.13.cloned.1.call-update) | async-done | bytes 131088 | tf_op jit(solution)/shard_map/reduce_scatter | solution.py:82
  142.4 6.6 %all_gather.18 = bf16[128,2048]{1,0:T(8,128)(2,1)S(1)} all-gather(bf16[32,2048]{1,0:T(8,128)(2,1)S(1)} %multiply_convert_fusion), channel_id=1, replica_groups=mesh['grp'=2,'sp'=4,'tp'=4] {'tp'}, dimensions={0}, use_global_device_ids=true | all-gather | bytes 655360 | tf_op jit(solution)/shard_map/all_gather | solution.py:44
  151.0 16.1 %all_gather.19 = bf16[512,512]{1,0:T(8,128)(2,1)S(1)} all-gather(bf16[128,512]{1,0:T(8,128)(2,1)S(1)} %fusion.67), channel_id=1, replica_groups=mesh['grp'=2,'sp'=4,'tp'=4] {'sp'}, dimensions={0}, use_global_device_ids=true | all-gather | bytes 655360 | tf_op jit(solution)/shard_map/all_gather | solution.py:51
  167.1 4.5 %multiply_reduce_fusion = (f32[4,512]{1,0:T(4,128)S(1)}, f32[4,512,1024]{2,1,0:T(8,128)}) fusion(bf16[1024,4,128]{0,2,1:T(8,128)(2,1)S(1)} %bitcast.104, bf16[512,512]{1,0:T(8,128)(2,1)S(1)} %all_gather.19), kind=kOutput, calls=%fused_computation.2 | convolution fusion | flops 541063168 | bytes 9969664 | tf_op jit(solution)/shard_map/qhd,khd->hqk/dot_general | solution.py:53
  171.5 12.3 %pmax.15 = f32[4,512]{1,0:T(4,128)S(1)} all-reduce(f32[4,512]{1,0:T(4,128)S(1)} %get-tuple-element.15), channel_id=1, replica_groups=mesh['grp'=2,'sp'=4,'tp'=4] {'sp'}, use_global_device_ids=true, to_apply=%region_10.0 | all-reduce | flops 2048 | bytes 16384 | tf_op jit(solution)/shard_map/pmax | solution.py:61
  183.9 4.4 %fusion.2 = bf16[4,512]{1,0:T(4,128)(2,1)S(1)} fusion(f32[4,512,1024]{2,1,0:T(8,128)} %get-tuple-element.16, f32[4,512]{1,0:T(4,128)S(1)} %pmax.15), kind=kLoop, calls=%fused_computation.6 | loop fusion | flops 6289408 | bytes 8400896 | tf_op jit(solution)/shard_map/reduce_sum | solution.py:74
  189.2 5.8 %fusion.61 = bf16[4,512,128]{2,1,0:T(8,128)(2,1)} fusion(bf16[1024,4,128]{0,2,1:T(8,128)(2,1)S(1)} %bitcast.106, f32[4,512,1024]{2,1,0:T(8,128)} %get-tuple-element.16, f32[4,512]{1,0:T(4,128)S(1)} %pmax.15), kind=kOutput, calls=%fused_computation.49 | convolution fusion | flops 543424512 | bytes 9969664 | tf_op jit(solution)/shard_map/hqk,khd->hqd/dot_general | solution.py:63
  195.0 11.5 %reduce-scatter.21.cloned.1.call-done = bf16[128,4]{1,0:T(8,128)(2,1)} async-done(((bf16[512,4]{1,0:T(8,128)(2,1)}), bf16[128,4]{1,0:T(8,128)(2,1)}) %reduce-scatter.21.cloned.1.call-update) | async-done | bytes 1040
  207.3 21.4 %reduce-scatter.15.cloned.1.call-done = bf16[4,128,128]{2,1,0:T(8,128)(2,1)} async-done(((bf16[4,512,128]{2,1,0:T(8,128)(2,1)}), bf16[4,128,128]{2,1,0:T(8,128)(2,1)}) %reduce-scatter.15.cloned.1.call-update) | async-done | bytes 131088 | tf_op jit(solution)/shard_map/reduce_scatter | solution.py:70
  229.8 2.9 %convolution_convert_fusion = bf16[128,2048]{1,0:T(8,128)(2,1)} fusion(bf16[128,512]{0,1:T(8,128)(2,1)S(1)} %bitcast.111, bf16[2,512,2048]{2,1,0:T(8,128)(2,1)} %param.12), kind=kOutput, calls=%fused_computation.14 | convolution fusion | flops 268697600 | bytes 2752512 | tf_op jit(solution)/shard_map/dot_general | solution.py:83
  232.7 20.0 %reduce-scatter.17.cloned.1.call-done = bf16[32,2048]{1,0:T(8,128)(2,1)} async-done(((bf16[128,2048]{1,0:T(8,128)(2,1)}), bf16[32,2048]{1,0:T(8,128)(2,1)}) %reduce-scatter.17.cloned.1.call-update) | async-done | bytes 131088 | tf_op jit(solution)/shard_map/reduce_scatter | solution.py:82
  (51 shorter events, 23.2 us)
Async XLA Ops:
  6.5 39.6 %all-gather.2.cloned.1.call-start = ((), (), s32[]{:S(2)}) async-start(), calls=%async_computation.6 | async-start | bytes 5242880 | tf_op jit(solution)/shard_map/all_gather | solution.py:28
  7.3 85.4 %reduce-scatter.19.cloned.1.call-start = ((), (), s32[]{:S(2)}) async-start(), calls=%async_computation.11 | async-start | bytes 163840
  46.1 5.4 %copy-start.2 = (bf16[2,2048,512]{2,1,0:T(8,128)(2,1)S(1)}, bf16[2,2048,512]{2,1,0:T(8,128)(2,1)}, u32[]{:S(2)}) copy-start(bf16[2,2048,512]{2,1,0:T(8,128)(2,1)} %param.10) | copy-start | bytes 12582916
  46.1 5.4 %copy-start.3 = (bf16[1024,2048]{1,0:T(8,128)(2,1)S(1)}, bf16[1024,2048]{1,0:T(8,128)(2,1)}, u32[]{:S(2)}) copy-start(bf16[1024,2048]{1,0:T(8,128)(2,1)} %all-gather.2.cloned.1.call-done) | copy-start | bytes 12582916
  75.8 39.2 %reduce-scatter.11.cloned.1.call-start = ((), (), s32[]{:S(2)}) async-start(), calls=%async_computation.7 | async-start | bytes 655360 | tf_op jit(solution)/shard_map/reduce_scatter | solution.py:70
  81.6 57.5 %reduce-scatter.13.cloned.1.call-start = ((), (), s32[]{:S(2)}) async-start(), calls=%async_computation.8 | async-start | bytes 655360 | tf_op jit(solution)/shard_map/reduce_scatter | solution.py:82
  119.1 87.4 %reduce-scatter.21.cloned.1.call-start = ((), (), s32[]{:S(2)}) async-start(), calls=%async_computation.12 | async-start | bytes 163840
  124.4 15.8 %copy-start = (bf16[32,2048]{1,0:T(8,128)(2,1)S(1)}, bf16[32,2048]{1,0:T(8,128)(2,1)}, u32[]{:S(2)}) copy-start(bf16[32,2048]{1,0:T(8,128)(2,1)} %param.7) | copy-start | bytes 393220
  189.1 39.6 %reduce-scatter.15.cloned.1.call-start = ((), (), s32[]{:S(2)}) async-start(), calls=%async_computation.9 | async-start | bytes 655360 | tf_op jit(solution)/shard_map/reduce_scatter | solution.py:70
  194.9 58.9 %copy-start.1 = (bf16[32,2048]{1,0:T(8,128)(2,1)S(1)}, bf16[32,2048]{1,0:T(8,128)(2,1)}, u32[]{:S(2)}) copy-start(bf16[32,2048]{1,0:T(8,128)(2,1)} %reduce-scatter.13.cloned.1.call-done) | copy-start | bytes 393220
  194.9 57.8 %reduce-scatter.17.cloned.1.call-start = ((), (), s32[]{:S(2)}) async-start(), calls=%async_computation.10 | async-start | bytes 655360 | tf_op jit(solution)/shard_map/reduce_scatter | solution.py:82
Sparse Core Ops, SparseCore 0:
  8.9 37.1 all-gather.1
  75.9 16.6 reduce-scatter.18
  94.9 20.0 reduce-scatter.10
  119.2 19.8 reduce-scatter.12
  189.2 17.1 reduce-scatter.20
  208.6 20.0 reduce-scatter.14
  232.8 19.8 reduce-scatter.16
where the time goes:
time: 263 us; the launch traced here: 262 us
  waiting for transfers between devices  104 us (40%)
  blocking collectives  71.8 us (27%)
  matrix products  48.7 us (19%)
  other arithmetic  19.3 us (7%)
  between operations  13.7 us (5%)
  local copies, waits for them, and re-layouts  4.73 us (2%)
    reduce_scatter x2, waiting for transfers between devices, body(): lax.psum_scatter(local_summed.astype(jnp.bfloat16), 'sp', scatter_dimensi...  42.9 us
    reduce_scatter x2, waiting for transfers between devices, body(): lax.psum_scatter(jnp.dot(attended, out_weight, preferred_element_type=jnp...  34.3 us
    all_gather x2, blocking collectives, body(): every_query = lax.all_gather(queries, 'sp', axis=0, tiled=True)  32.4 us
    pmax x2, blocking collectives, body(): row_peak = lax.pmax(jnp.max(scores, axis=2), 'sp')  24.2 us
    unnamed x9, waiting for transfers between devices  17.8 us
    all_gather x2, blocking collectives, body(): lax.all_gather(normed, 'tp', axis=0, tiled=True)  15.2 us
    dot_general x2, matrix products, body(): jnp.einsum('hqk,khd->hqd', weights.astype(jnp.bfloat16), split_heads(valu...  11.5 us
    dot_general x2, matrix products, body(): jnp.dot(project_shard_part, w_value[level], preferred_element_type=jnp.fl...  10.6 us
  transfers between devices with their start and end apart: 7, of which 7 were waited for; matrix products, arithmetic and copies ran while one was open for 11% of the time, Pallas kernels for 0%

commit v1 on v0

--- a/solution.py
+++ b/solution.py
@@ -1,12 +1,21 @@
+import functools
+import math
+
 import jax
 import jax.numpy as jnp
 from jax import lax
+from jax.experimental import pallas as pl
+from jax.experimental.pallas import tpu as pltpu
 from jax.sharding import PartitionSpec as P
 
 HEAD = 128
+CORES = 2
 
 
 EPS = 1e-06
+MESH = pl.DeviceIdType.MESH
+F32 = jnp.float32
+BF16 = jnp.bfloat16
 
 
 def normalize(row_block, gain_row):
@@ -15,6 +24,350 @@
         * lax.rsqrt(jnp.mean(row_block * row_block, axis=-1, keepdims=True) + EPS)
         * gain_row
     )
+
+
+def fused_kernel(
+    nx, sp, depth,
+    target, source, w_query, w_key, w_value, w_out, gains, out,
+    tbuf, sbuf, wq, wk, wv, wo, keys, values, stream, normed, qbuf,
+    osend, orecv, ssend, srecv, attended, pbuf, half_in, chip_sum, fin,
+    local_sem, weight_sem, t_send, t_recv, t_fsend, s_psend, s_send, s_recv, s_fsend,
+    q_send, q_recv, o_send, o_recv, e_send, e_recv,
+    h_send, h_recv, c_send, c_psend, c_fsend, c_recv, c_frecv, f_send, f_recv,
+):
+    s = lax.axis_index("sp")
+    t = lax.axis_index("tp")
+    x = t // CORES
+    c = t % CORES
+    partner_c = 1 - c
+    partner = {"tp": x * CORES + partner_c}
+    units = sbuf.shape[0]
+    half = sbuf.shape[2]
+    width = sbuf.shape[3]
+    rows = 2 * half
+    local_width = wk.shape[2]
+    heads = local_width // HEAD
+    tp = nx * CORES
+    trows = tbuf.shape[1]
+    score_scale = HEAD ** (-0.5) * math.log2(math.e)
+
+    def chip(step):
+        return lax.rem(x + step, nx)
+
+    def peer(step):
+        return {"tp": chip(step) * CORES + c}
+
+    def remote(src, dst, send_sem, recv_sem, device):
+        return pltpu.make_async_remote_copy(
+            src_ref=src, dst_ref=dst, send_sem=send_sem, recv_sem=recv_sem,
+            device_id=device, device_id_type=MESH,
+        )
+
+    def arrived(dst, recv_sem):
+        remote(dst, dst, t_send.at[0], recv_sem, partner).wait_recv()
+
+    own_target = pltpu.make_async_copy(target, tbuf.at[t], local_sem.at[0])
+    own_source = [
+        pltpu.make_async_copy(
+            source.at[pl.ds(part * half, half)], sbuf.at[0, part], local_sem.at[1 + part])
+        for part in range(2)
+    ]
+
+    def load(kind, level):
+        pair = ((w_query, wq), (w_key, wk), (w_value, wv), (w_out, wo))[kind]
+        return pltpu.make_async_copy(
+            pair[0].at[level], pair[1].at[level], weight_sem.at[kind, level])
+
+    own_target.start()
+    for copy in own_source:
+        copy.start()
+    load(1, 0).start()
+    load(2, 0).start()
+
+    barrier = pltpu.get_barrier_semaphore()
+    pl.semaphore_signal(barrier, inc=1, device_id=partner, device_id_type=MESH)
+    for step in range(1, nx):
+        pl.semaphore_signal(barrier, inc=1, device_id=peer(step), device_id_type=MESH)
+    for step in range(1, sp):
+        pl.semaphore_signal(
+            barrier, inc=1, device_id={"sp": lax.rem(s + step, sp)}, device_id_type=MESH)
+    pl.semaphore_wait(barrier, 1 + (nx - 1) + (sp - 1))
+
+    sends = []
+
+    def go(copy):
+        copy.start()
+        sends.append(copy)
+
+    for step in range(1, nx):
+        go(remote(target, tbuf.at[t], t_send.at[step], t_recv.at[t], peer(step)))
+    go(remote(target, tbuf.at[t], t_send.at[0], t_recv.at[t], partner))
+    for part in range(2):
+        block = source.at[pl.ds(part * half, half)]
+        for step in range(1, nx):
+            unit = 2 * (nx - step) + part
+            go(remote(block, sbuf.at[unit, 0], s_send.at[step, part], s_recv.at[unit, 0], peer(step)))
+        go(remote(block, sbuf.at[1, part], s_psend.at[part], s_recv.at[1, part], partner))
+
+    def project(index):
+        unit = index // depth
+        level = index % depth
+        block = sbuf[unit].reshape(rows, width)
+        start = pl.multiple_of(unit * rows, rows)
+        k = jnp.dot(block, wk[level], preferred_element_type=F32)
+        keys[level, pl.ds(start, rows), :] = k.astype(BF16)
+        v = jnp.dot(block, wv[level], preferred_element_type=F32)
+        values[level, :, pl.ds(start, rows)] = v.T.astype(BF16)
+
+    def make_queries(level):
+        q = jnp.dot(normed[...].reshape(tp * trows, width), wq[level], preferred_element_type=F32)
+        qbuf[level, s] = q.astype(BF16)
+        for step in range(1, sp):
+            dest = lax.rem(s + step, sp)
+            remote(qbuf.at[level, s], qbuf.at[level, s], q_send.at[level, step],
+                   q_recv.at[level, s], {"sp": dest}).start()
+
+    def first_queries():
+        own_target.wait()
+        for step in range(1, nx):
+            slot = chip(step) * CORES + c
+            arrived(tbuf.at[slot], t_recv.at[slot])
+            remote(tbuf.at[slot], tbuf.at[slot], t_fsend.at[step], t_recv.at[slot], partner).start()
+        for step in range(nx):
+            slot = chip(step) * CORES + partner_c
+            arrived(tbuf.at[slot], t_recv.at[slot])
+
+        @pl.loop(0, tp)
+        def _(block):
+            value = tbuf[block].astype(F32)
+            stream[block] = value
+            normed[block] = normalize(value, gains[0, 0:1, :]).astype(BF16)
+
+        load(0, 0).wait()
+        make_queries(0)
+
+    @pl.loop(0, units * depth - (depth - 1))
+    def _(index):
+        unit = index // depth
+        level = index % depth
+
+        @pl.when(index == 0)
+        def _():
+            for copy in own_source:
+                copy.wait()
+            load(1, 0).wait()
+            load(2, 0).wait()
+            load(0, 0).start()
+            for later in range(1, depth):
+                load(1, later).start()
+                load(2, later).start()
+            load(3, 0).start()
+            for later in range(1, depth):
+                load(0, later).start()
+                load(3, later).start()
+
+        for later in range(1, depth):
+            @pl.when(index == later)
+            def _():
+                load(1, later).wait()
+                load(2, later).wait()
+
+        @pl.when(index == depth)
+        def _():
+            first_queries()
+            for part in range(2):
+                arrived(sbuf.at[1, part], s_recv.at[1, part])
+
+        @pl.when(jnp.logical_and(unit >= 2, level == 0))
+        def _():
+            arrived(sbuf.at[unit, 0], s_recv.at[unit, 0])
+            remote(sbuf.at[unit, 0], sbuf.at[unit, 1], s_fsend.at[unit],
+                   s_recv.at[unit, 1], partner).start()
+            arrived(sbuf.at[unit, 1], s_recv.at[unit, 1])
+
+        project(index)
+
+    both = jnp.minimum(s, sp - 1 - s)
+
+    def near(i):
+        side = jnp.where(i % 2 == 1, s - (i + 1) // 2, s + i // 2)
+        rest = jnp.where(s < sp - 1 - s, i, sp - 1 - i)
+        return jnp.where(i <= 2 * both, side, rest)
+
+    for layer in range(depth):
+        last = layer == depth - 1
+
+        @pl.loop(0, sp)
+        def _(i):
+            j = near(i)
+
+            @pl.when(j != s)
+            def _():
+                arrived(qbuf.at[layer, j], q_recv.at[layer, j])
+
+            q = qbuf[layer, j]
+            peaks, totals = [], []
+            for h in range(heads):
+                cols = slice(h * HEAD, (h + 1) * HEAD)
+                scores = lax.dot_general(
+                    keys[layer, :, cols], q[:, cols], (((1,), (1,)), ((), ())),
+                    preferred_element_type=F32)
+                peak = jnp.max(scores, axis=0, keepdims=True) * score_scale
+                weights = jnp.exp2(scores * score_scale - peak)
+                totals.append(jnp.sum(weights, axis=0, keepdims=True))
+                peaks.append(peak)
+                o = jnp.dot(values[layer, cols, :], weights.astype(BF16), preferred_element_type=F32)
+                osend[layer, j, cols, :] = o.astype(BF16)
+            ssend[layer, j] = jnp.concatenate(peaks + totals, axis=0)
+
+            @pl.when(j != s)
+            def _():
+                remote(osend.at[layer, j], orecv.at[layer, s], o_send.at[layer, j],
+                       o_recv.at[layer, s], {"sp": j}).start()
+                remote(ssend.at[layer, j], srecv.at[layer, s], e_send.at[layer, j],
+                       e_recv.at[layer, s], {"sp": j}).start()
+
+            @pl.when(j == s)
+            def _():
+                orecv[layer, s] = osend[layer, s]
+                srecv[layer, s] = ssend[layer, s]
+
+        if layer == 0:
+            @pl.loop(units * depth - (depth - 1), units * depth)
+            def _(index):
+                project(index)
+        load(3, layer).wait()
+
+        for step in range(1, sp):
+            j = lax.rem(s + step, sp)
+            arrived(orecv.at[layer, j], o_recv.at[layer, j])
+            arrived(srecv.at[layer, j], e_recv.at[layer, j])
+        peaks = [srecv[layer, j, 0:heads, :] for j in range(sp)]
+        top = functools.reduce(jnp.maximum, peaks)
+        share = [jnp.exp2(p - top) for p in peaks]
+        total = sum(share[j] * srecv[layer, j, heads:2 * heads, :] for j in range(sp))
+        share = [one / total for one in share]
+        for h in range(heads):
+            cols = slice(h * HEAD, (h + 1) * HEAD)
+            mixed = sum(share[j][h:h + 1, :] * orecv[layer, j, cols, :].astype(F32) for j in range(sp))
+            attended[:, cols] = mixed.T.astype(BF16)
+
+        tile = min(512, width)
+        for n in range(width // tile):
+            cols = slice(n * tile, (n + 1) * tile)
+            part = jnp.dot(attended[...], wo[layer, :, cols], preferred_element_type=F32)
+            pbuf[layer, :, :, :, cols] = part.astype(BF16).reshape(nx, CORES, trows, tile)
+
+        go(remote(pbuf.at[layer, :, partner_c], half_in.at[layer], h_send.at[layer],
+                  h_recv.at[layer], partner))
+        arrived(half_in.at[layer], h_recv.at[layer])
+        if not last:
+            for b in range(nx):
+                both_cores = pbuf[layer, b, c].astype(F32) + half_in[layer, b].astype(F32)
+                chip_sum[layer, x, c, b] = both_cores.astype(BF16)
+            own = chip_sum.at[layer, x, c]
+            for step in range(1, nx):
+                go(remote(own, own, c_send.at[layer, step], c_recv.at[layer, x], peer(step)))
+            go(remote(own, own, c_psend.at[layer], c_frecv.at[layer, x], partner))
+            for step in range(1, nx):
+                other = chip_sum.at[layer, chip(step), c]
+                arrived(other, c_recv.at[layer, chip(step)])
+                go(remote(other, other, c_fsend.at[layer, step], c_frecv.at[layer, chip(step)], partner))
+            for step in range(nx):
+                arrived(chip_sum.at[layer, chip(step), partner_c], c_frecv.at[layer, chip(step)])
+            load(0, layer + 1).wait()
+
+            @pl.loop(0, tp)
+            def _(block):
+                projected = sum(
+                    chip_sum[layer, a, block % CORES, block // CORES].astype(F32) for a in range(nx))
+                value = stream[block] + normalize(projected, gains[layer, 1:2, :])
+                stream[block] = value
+                normed[block] = normalize(value, gains[layer + 1, 0:1, :]).astype(BF16)
+
+            make_queries(layer + 1)
+        else:
+            for step in range(1, nx):
+                b = chip(step)
+                both_cores = pbuf[layer, b, c].astype(F32) + half_in[layer, b].astype(F32)
+                fin[0, b] = both_cores.astype(BF16)
+                go(remote(fin.at[0, b], fin.at[1, x], f_send.at[step], f_recv.at[x], peer(step)))
+            projected = pbuf[layer, x, c].astype(F32) + half_in[layer, x].astype(F32)
+            for step in range(1, nx):
+                b = chip(step)
+                arrived(fin.at[1, b], f_recv.at[b])
+                projected = projected + fin[1, b].astype(F32)
+            value = stream[t] + normalize(projected, gains[layer, 1:2, :])
+            out[...] = value.astype(out.dtype)
+
+    for copy in sends:
+        copy.wait_send()
+    for step in range(1, nx):
+        slot = chip(step) * CORES + c
+        remote(tbuf.at[slot], tbuf.at[slot], t_fsend.at[step], t_recv.at[slot], partner).wait_send()
+    for unit in range(2, units):
+        remote(sbuf.at[unit, 0], sbuf.at[unit, 1], s_fsend.at[unit],
+               s_recv.at[unit, 1], partner).wait_send()
+    for layer in range(depth):
+        for step in range(1, sp):
+            j = lax.rem(s + step, sp)
+            remote(qbuf.at[layer, s], qbuf.at[layer, s], q_send.at[layer, step],
+                   q_recv.at[layer, s], {"sp": j}).wait_send()
+            remote(osend.at[layer, j], orecv.at[layer, s], o_send.at[layer, j],
+                   o_recv.at[layer, s], {"sp": j}).wait_send()
+            remote(ssend.at[layer, j], srecv.at[layer, s], e_send.at[layer, j],
+                   e_recv.at[layer, s], {"sp": j}).wait_send()
+
+
+def fused_body(nx, sp, target, source, w_query, w_key, w_value, w_out, gains):
+    depth, width, local_width = w_query.shape
+    trows, rows = target.shape[0], source.shape[0]
+    tp = nx * CORES
+    block_rows = tp * trows
+    heads = local_width // HEAD
+    units = 2 * nx
+    vmem = pltpu.VMEM
+    dma = pltpu.SemaphoreType.DMA
+    anywhere = pl.BlockSpec(memory_space=pl.ANY)
+    whole = pl.BlockSpec(memory_space=pltpu.VMEM)
+    return pl.pallas_call(
+        functools.partial(fused_kernel, nx, sp, depth),
+        out_shape=jax.ShapeDtypeStruct((trows, width), BF16),
+        in_specs=[anywhere] * 6 + [whole],
+        out_specs=whole,
+        scratch_shapes=[
+            vmem((tp, trows, width), BF16),
+            vmem((units, 2, rows // 2, width), BF16),
+            vmem(w_query.shape, BF16),
+            vmem(w_key.shape, BF16),
+            vmem(w_value.shape, BF16),
+            vmem(w_out.shape, BF16),
+            vmem((depth, units * rows, local_width), BF16),
+            vmem((depth, local_width, units * rows), BF16),
+            vmem((tp, trows, width), F32),
+            vmem((tp, trows, width), BF16),
+            vmem((depth, sp, block_rows, local_width), BF16),
+            vmem((depth, sp, local_width, block_rows), BF16),
+            vmem((depth, sp, local_width, block_rows), BF16),
+            vmem((depth, sp, 2 * heads, block_rows), F32),
+            vmem((depth, sp, 2 * heads, block_rows), F32),
+            vmem((block_rows, local_width), BF16),
+            vmem((depth, nx, CORES, trows, width), BF16),
+            vmem((depth, nx, trows, width), BF16),
+            vmem((depth, nx, CORES, nx, trows, width), BF16),
+            vmem((2, nx, trows, width), BF16),
+            dma((3,)), dma((4, depth)),
+            dma((nx,)), dma((tp,)), dma((nx,)),
+            dma((2,)), dma((nx, 2)), dma((units, 2)), dma((units,)),
+            dma((depth, sp)), dma((depth, sp)),
+            dma((depth, sp)), dma((depth, sp)), dma((depth, sp)), dma((depth, sp)),
+            dma((depth,)), dma((depth,)),
+            dma((depth, nx)), dma((depth,)), dma((depth, nx)), dma((depth, nx)), dma((depth, nx)),
+            dma((nx,)), dma((nx,)),
+        ],
+        compiler_params=pltpu.CompilerParams(
+            collective_id=0, has_side_effects=True, vmem_limit_bytes=60 * 1024 * 1024),
+    )(target, source, w_query, w_key, w_value, w_out, gains)
 
 
 def split_heads(row_block):
@@ -100,4 +453,13 @@
         P(),
     )
     out_specs = P(("grp", "sp", "tp"), None)
-    return jax.shard_map(body, mesh=mesh, in_specs=in_specs, out_specs=out_specs, check_vma=False)
+    sp, tp = mesh.shape["sp"], mesh.shape["tp"]
+
+    def run(target, source, w_query, w_key, w_value, w_out, gains):
+        trows, rows, local_width = target.shape[0], source.shape[0], w_query.shape[2]
+        tiles = (trows % 16 == 0 and (tp * trows) % 128 == 0 and rows % 128 == 0
+                 and local_width % (4 * HEAD) == 0 and tp % CORES == 0)
+        form = functools.partial(fused_body, tp // CORES, sp) if tiles else body
+        return form(target, source, w_query, w_key, w_value, w_out, gains)
+
+    return jax.shard_map(run, mesh=mesh, in_specs=in_specs, out_specs=out_specs, check_vma=False)

time: 263 us -> 97.9 us (0.37)
  waiting for transfers between devices: 104 us -> 0 us
  Pallas kernels: 0 us -> 96.1 us
  blocking collectives: 71.8 us -> 0 us
  matrix products: 48.7 us -> 0 us
  other arithmetic: 19.3 us -> 0 us
  between operations: 13.7 us -> 0.01 us
  local copies, waits for them, and re-layouts: 4.73 us -> 1.57 us
    pallas_call x0 -> x1, Pallas kernels: none -> 96.1 us  [fused_body(): pl.pallas_call(functools.partial(fused_kernel, nx, sp, depth), out_shape=...]
    reduce_scatter x4 -> x0, waiting for transfers between devices: 77.2 us -> none  [the longest x2 42.9 us: body(): lax.psum_scatter(local_summed.astype(jnp.bfloat16), 'sp', scatter_dimensi...]
    dot_general x12 -> x0, matrix products: 48.7 us -> none  [the longest x2 11.5 us: body(): jnp.einsum('hqk,khd->hqd', weights.astype(jnp.bfloat16), split_heads(valu...]
    all_gather x4 -> x0, blocking collectives: 47.6 us -> none  [the longest x2 32.4 us: body(): every_query = lax.all_gather(queries, 'sp', axis=0, tiled=True)]
    pmax x2 -> x0, blocking collectives: 24.2 us -> none  [body(): row_peak = lax.pmax(jnp.max(scores, axis=2), 'sp')]
    unnamed x9 -> x0, waiting for transfers between devices: 17.8 us -> none
    reduce_sum x6 -> x0, other arithmetic: 13 us -> none  [the longest x2 8.74 us: body(): jnp.sum(weights, axis=2).astype(jnp.bfloat16)]
    all_gather x1 -> x0, waiting for transfers between devices: 8.73 us -> none  [body(): project_shard_part = lax.all_gather(source, 'tp', axis=0, tiled=True)]
  transfers between devices with their start and end apart: 7 -> 0, of which waited for: 7 -> 0; matrix products, arithmetic and copies ran while one was open for 11% -> 0% of each run, Pallas kernels for 0% -> 0%
where the time goes in v1:
time: 97.9 us; the launch traced here: 97.7 us
  Pallas kernels  96.1 us (98%)
  local copies, waits for them, and re-layouts  1.57 us (2%)
    pallas_call x1, Pallas kernels, fused_body(): pl.pallas_call(functools.partial(fused_kernel, nx, sp, depth), out_shape=...  96.1 us

profile of v1, /device:TPU:0, one launch (start us, length us, event | category | flops | bytes accessed | tf_op | source)
XLA Modules:
  0.0 97.7 jit_solution(12265889198747801282)
XLA Ops:
  0.0 96.1 %shard_map.73 = bf16[32,2048]{1,0:T(8,128)(2,1)} custom-call(bf16[32,2048]{1,0:T(8,128)(2,1)} %target.1, bf16[256,2048]{1,0:T(8,128)(2,1)} %source.1, bf16[2,2048,512]{2,1,0:T(8,128)(2,1)} %w_query.1, bf16[2,2048,512]{2,1,0:T(8,128)(2,1)} %w_key.1, bf16[2,2048,512]{2,1,0:T(8,128)(2,1)} %w_value.1, bf16[2,512,2048]{2,1,0:T(8,128)(2,1)} %w_out.1, ...), custom_call_target="tpu_custom_call" | custom-call | tf_op jit(solution)/shard_map/pallas_call | solution.py:333
  96.1 1.6 %copy.9 = bf16[32,2048]{1,0:T(8,128)(2,1)} copy(bf16[32,2048]{1,0:T(8,128)(2,1)} %shard_map.73) | data formatting | bytes 262144

commit v2 on v1

--- a/solution.py
+++ b/solution.py
@@ -95,6 +95,14 @@
 
     sends = []
 
+    drains = []
+
+    def finish():
+        for drain in drains:
+            drain()
+        for copy in sends:
+            copy.wait_send()
+
     def go(copy):
         copy.start()
         sends.append(copy)
@@ -104,9 +112,12 @@
     go(remote(target, tbuf.at[t], t_send.at[0], t_recv.at[t], partner))
     for part in range(2):
         block = source.at[pl.ds(part * half, half)]
-        for step in range(1, nx):
-            unit = 2 * (nx - step) + part
-            go(remote(block, sbuf.at[unit, 0], s_send.at[step, part], s_recv.at[unit, 0], peer(step)))
+        for piece in range(2):
+            span = pl.ds(piece * (half // 2), half // 2)
+            for step in range(1, nx):
+                unit = 2 * (nx - step) + part
+                go(remote(block.at[span], sbuf.at[unit, 0, span], s_send.at[step, 2 * part + piece],
+                          s_recv.at[unit, piece], peer(step)))
         go(remote(block, sbuf.at[1, part], s_psend.at[part], s_recv.at[1, part], partner))
 
     def project(index):
@@ -119,20 +130,55 @@
         v = jnp.dot(block, wv[level], preferred_element_type=F32)
         values[level, :, pl.ds(start, rows)] = v.T.astype(BF16)
 
+    def query_copy(level, step):
+        return remote(qbuf.at[level, s], qbuf.at[level, s], q_send.at[level, step],
+                      q_recv.at[level, s], {"sp": lax.rem(s + step, sp)})
+
+    def drain_queries(level):
+        for step in range(1, sp):
+            query_copy(level, step).wait_send()
+
+    def result_copies(level, j):
+        return (
+            remote(osend.at[level, j], orecv.at[level, s], o_send.at[level, j],
+                   o_recv.at[level, s], {"sp": j}),
+            remote(ssend.at[level, j], srecv.at[level, s], e_send.at[level, j],
+                   e_recv.at[level, s], {"sp": j}),
+        )
+
+    def drain_results(level):
+        for step in range(1, sp):
+            for copy in result_copies(level, lax.rem(s + step, sp)):
+                copy.wait_send()
+
+    def target_relay(step):
+        slot = chip(step) * CORES + c
+        return remote(tbuf.at[slot], tbuf.at[slot], t_fsend.at[step], t_recv.at[slot], partner)
+
+    def source_relay(unit, piece):
+        span = pl.ds(piece * (half // 2), half // 2)
+        return remote(sbuf.at[unit, 0, span], sbuf.at[unit, 1, span], s_fsend.at[unit, piece],
+                      s_recv.at[unit, 2 + piece], partner)
+
+    def drain_relays():
+        for step in range(1, nx):
+            target_relay(step).wait_send()
+        for unit in range(2, units):
+            for piece in range(2):
+                source_relay(unit, piece).wait_send()
+
     def make_queries(level):
         q = jnp.dot(normed[...].reshape(tp * trows, width), wq[level], preferred_element_type=F32)
         qbuf[level, s] = q.astype(BF16)
         for step in range(1, sp):
-            dest = lax.rem(s + step, sp)
-            remote(qbuf.at[level, s], qbuf.at[level, s], q_send.at[level, step],
-                   q_recv.at[level, s], {"sp": dest}).start()
+            query_copy(level, step).start()
 
     def first_queries():
         own_target.wait()
         for step in range(1, nx):
             slot = chip(step) * CORES + c
             arrived(tbuf.at[slot], t_recv.at[slot])
-            remote(tbuf.at[slot], tbuf.at[slot], t_fsend.at[step], t_recv.at[slot], partner).start()
+            target_relay(step).start()
         for step in range(nx):
             slot = chip(step) * CORES + partner_c
             arrived(tbuf.at[slot], t_recv.at[slot])
@@ -180,12 +226,17 @@
 
         @pl.when(jnp.logical_and(unit >= 2, level == 0))
         def _():
-            arrived(sbuf.at[unit, 0], s_recv.at[unit, 0])
-            remote(sbuf.at[unit, 0], sbuf.at[unit, 1], s_fsend.at[unit],
-                   s_recv.at[unit, 1], partner).start()
-            arrived(sbuf.at[unit, 1], s_recv.at[unit, 1])
+            for piece in range(2):
+                span = pl.ds(piece * (half // 2), half // 2)
+                arrived(sbuf.at[unit, 0, span], s_recv.at[unit, piece])
+                source_relay(unit, piece).start()
+            for piece in range(2):
+                span = pl.ds(piece * (half // 2), half // 2)
+                arrived(sbuf.at[unit, 1, span], s_recv.at[unit, 2 + piece])
 
         project(index)
+
+    drains += [drain_relays, functools.partial(drain_queries, 0)]
 
     both = jnp.minimum(s, sp - 1 - s)
 
@@ -199,7 +250,7 @@
 
         @pl.loop(0, sp)
         def _(i):
-            j = near(i)
+            j = near(sp - 1 - i if layer == 0 else i)
 
             @pl.when(j != s)
             def _():
@@ -222,16 +273,15 @@
 
             @pl.when(j != s)
             def _():
-                remote(osend.at[layer, j], orecv.at[layer, s], o_send.at[layer, j],
-                       o_recv.at[layer, s], {"sp": j}).start()
-                remote(ssend.at[layer, j], srecv.at[layer, s], e_send.at[layer, j],
-                       e_recv.at[layer, s], {"sp": j}).start()
+                for copy in result_copies(layer, j):
+                    copy.start()
 
             @pl.when(j == s)
             def _():
                 orecv[layer, s] = osend[layer, s]
                 srecv[layer, s] = ssend[layer, s]
 
+        drains.append(functools.partial(drain_results, layer))
         if layer == 0:
             @pl.loop(units * depth - (depth - 1), units * depth)
             def _(index):
@@ -258,23 +308,31 @@
             part = jnp.dot(attended[...], wo[layer, :, cols], preferred_element_type=F32)
             pbuf[layer, :, :, :, cols] = part.astype(BF16).reshape(nx, CORES, trows, tile)
 
-        go(remote(pbuf.at[layer, :, partner_c], half_in.at[layer], h_send.at[layer],
-                  h_recv.at[layer], partner))
-        arrived(half_in.at[layer], h_recv.at[layer])
+        order = [chip(step) for step in list(range(1, nx)) + [0]]
+        for b in order:
+            go(remote(pbuf.at[layer, b, partner_c], half_in.at[layer, b], h_send.at[layer, b],
+                      h_recv.at[layer, b], partner))
         if not last:
-            for b in range(nx):
+            for k, b in enumerate(order):
+                arrived(half_in.at[layer, b], h_recv.at[layer, b])
                 both_cores = pbuf[layer, b, c].astype(F32) + half_in[layer, b].astype(F32)
                 chip_sum[layer, x, c, b] = both_cores.astype(BF16)
-            own = chip_sum.at[layer, x, c]
+                own = chip_sum.at[layer, x, c, b]
+                for step in range(1, nx):
+                    go(remote(own, own, c_send.at[layer, step, k], c_recv.at[layer, x, b], peer(step)))
+                go(remote(own, own, c_psend.at[layer, k], c_frecv.at[layer, x, b], partner))
             for step in range(1, nx):
-                go(remote(own, own, c_send.at[layer, step], c_recv.at[layer, x], peer(step)))
-            go(remote(own, own, c_psend.at[layer], c_frecv.at[layer, x], partner))
-            for step in range(1, nx):
-                other = chip_sum.at[layer, chip(step), c]
-                arrived(other, c_recv.at[layer, chip(step)])
-                go(remote(other, other, c_fsend.at[layer, step], c_frecv.at[layer, chip(step)], partner))
+                a = chip(step)
+                for k in range(nx):
+                    b = lax.rem(a + 1 + k, nx)
+                    other = chip_sum.at[layer, a, c, b]
+                    arrived(other, c_recv.at[layer, a, b])
+                    go(remote(other, other, c_fsend.at[layer, step, k], c_frecv.at[layer, a, b], partner))
             for step in range(nx):
-                arrived(chip_sum.at[layer, chip(step), partner_c], c_frecv.at[layer, chip(step)])
+                a = chip(step)
+                for k in range(nx):
+                    b = lax.rem(a + 1 + k, nx)
+                    arrived(chip_sum.at[layer, a, partner_c, b], c_frecv.at[layer, a, b])
             load(0, layer + 1).wait()
 
             @pl.loop(0, tp)
@@ -286,12 +344,15 @@
                 normed[block] = normalize(value, gains[layer + 1, 0:1, :]).astype(BF16)
 
             make_queries(layer + 1)
+            drains.append(functools.partial(drain_queries, layer + 1))
         else:
             for step in range(1, nx):
                 b = chip(step)
+                arrived(half_in.at[layer, b], h_recv.at[layer, b])
                 both_cores = pbuf[layer, b, c].astype(F32) + half_in[layer, b].astype(F32)
                 fin[0, b] = both_cores.astype(BF16)
                 go(remote(fin.at[0, b], fin.at[1, x], f_send.at[step], f_recv.at[x], peer(step)))
+            arrived(half_in.at[layer, x], h_recv.at[layer, x])
             projected = pbuf[layer, x, c].astype(F32) + half_in[layer, x].astype(F32)
             for step in range(1, nx):
                 b = chip(step)
@@ -300,23 +361,7 @@
             value = stream[t] + normalize(projected, gains[layer, 1:2, :])
             out[...] = value.astype(out.dtype)
 
-    for copy in sends:
-        copy.wait_send()
-    for step in range(1, nx):
-        slot = chip(step) * CORES + c
-        remote(tbuf.at[slot], tbuf.at[slot], t_fsend.at[step], t_recv.at[slot], partner).wait_send()
-    for unit in range(2, units):
-        remote(sbuf.at[unit, 0], sbuf.at[unit, 1], s_fsend.at[unit],
-               s_recv.at[unit, 1], partner).wait_send()
-    for layer in range(depth):
-        for step in range(1, sp):
-            j = lax.rem(s + step, sp)
-            remote(qbuf.at[layer, s], qbuf.at[layer, s], q_send.at[layer, step],
-                   q_recv.at[layer, s], {"sp": j}).wait_send()
-            remote(osend.at[layer, j], orecv.at[layer, s], o_send.at[layer, j],
-                   o_recv.at[layer, s], {"sp": j}).wait_send()
-            remote(ssend.at[layer, j], srecv.at[layer, s], e_send.at[layer, j],
-                   e_recv.at[layer, s], {"sp": j}).wait_send()
+    finish()
 
 
 def fused_body(nx, sp, target, source, w_query, w_key, w_value, w_out, gains):
@@ -358,11 +403,12 @@
             vmem((2, nx, trows, width), BF16),
             dma((3,)), dma((4, depth)),
             dma((nx,)), dma((tp,)), dma((nx,)),
-            dma((2,)), dma((nx, 2)), dma((units, 2)), dma((units,)),
+            dma((2,)), dma((nx, 4)), dma((units, 4)), dma((units, 2)),
             dma((depth, sp)), dma((depth, sp)),
             dma((depth, sp)), dma((depth, sp)), dma((depth, sp)), dma((depth, sp)),
-            dma((depth,)), dma((depth,)),
-            dma((depth, nx)), dma((depth,)), dma((depth, nx)), dma((depth, nx)), dma((depth, nx)),
+            dma((depth, nx)), dma((depth, nx)),
+            dma((depth, nx, nx)), dma((depth, nx)), dma((depth, nx, nx)),
+            dma((depth, nx, nx)), dma((depth, nx, nx)),
             dma((nx,)), dma((nx,)),
         ],
         compiler_params=pltpu.CompilerParams(
@@ -457,7 +503,7 @@
 
     def run(target, source, w_query, w_key, w_value, w_out, gains):
         trows, rows, local_width = target.shape[0], source.shape[0], w_query.shape[2]
-        tiles = (trows % 16 == 0 and (tp * trows) % 128 == 0 and rows % 128 == 0
+        tiles = (trows % 16 == 0 and (tp * trows) % 128 == 0 and rows % 128 == 0 and rows % 64 == 0
                  and local_width % (4 * HEAD) == 0 and tp % CORES == 0)
         form = functools.partial(fused_body, tp // CORES, sp) if tiles else body
         return form(target, source, w_query, w_key, w_value, w_out, gains)

time: 97.9 us -> 96.5 us (0.986)
  Pallas kernels: 96.1 us -> 94.8 us
    pallas_call x1, Pallas kernels: 96.1 us -> 94.8 us  [fused_body(): pl.pallas_call(functools.partial(fused_kernel, nx, sp, depth), out_shape=...]
where the time goes in v2:
time: 96.5 us; the launch traced here: 96.3 us
  Pallas kernels  94.8 us (98%)
  local copies, waits for them, and re-layouts  1.57 us (2%)
    pallas_call x1, Pallas kernels, fused_body(): pl.pallas_call(functools.partial(fused_kernel, nx, sp, depth), out_shape=...  94.8 us

profile of v2, /device:TPU:0, one launch (start us, length us, event | category | flops | bytes accessed | tf_op | source)
XLA Modules:
  0.0 96.3 jit_solution(3763415107744869442)
XLA Ops:
  0.0 94.8 %shard_map.73 = bf16[32,2048]{1,0:T(8,128)(2,1)} custom-call(bf16[32,2048]{1,0:T(8,128)(2,1)} %target.1, bf16[256,2048]{1,0:T(8,128)(2,1)} %source.1, bf16[2,2048,512]{2,1,0:T(8,128)(2,1)} %w_query.1, bf16[2,2048,512]{2,1,0:T(8,128)(2,1)} %w_key.1, bf16[2,2048,512]{2,1,0:T(8,128)(2,1)} %w_value.1, bf16[2,512,2048]{2,1,0:T(8,128)(2,1)} %w_out.1, ...), custom_call_target="tpu_custom_call" | custom-call | tf_op jit(solution)/shard_map/pallas_call | solution.py:378
  94.8 1.6 %copy.9 = bf16[32,2048]{1,0:T(8,128)(2,1)} copy(bf16[32,2048]{1,0:T(8,128)(2,1)} %shard_map.73) | data formatting | bytes 262144
